TPU v7x, 32 devices: a whole 2x2x4 slice. The times are simulated.
32 devices in a mesh: sp: 16 (over z, y, x), tp: 2 (over core).
Axes of the slice: x: 2, y: 2, z: 4, core: 2. Of those that a mesh axis runs over, the one named last changes fastest.
Arguments:
- tokens: bfloat16 [6144, 2048], P(('sp', 'tp')), may hold values from -6 to 6
- query_weight: bfloat16 [2048, 1024], P(None, 'tp'), may hold values from -0.125 to 0.125
- key_weight: bfloat16 [2048, 1024], P(None, 'tp'), may hold values from -0.125 to 0.125
- value_weight: bfloat16 [2048, 1024], P(None, 'tp'), may hold values from -0.125 to 0.125
- query_gain: float32 [64], replicated, may hold values from 0.5 to 16
- key_gain: float32 [64], replicated, may hold values from 0.5 to 16
- log_gate_total: float32 [6144, 16], P('sp', 'tp'), may hold values from -877 to 0, as said below
- output_weight: bfloat16 [1024, 2048], P('tp'), may hold values from -0.1875 to 0.1875
Outputs:
- mixed: bfloat16 [6144, 2048], P(('sp', 'tp'))
Inputs may be any that keep to these rules, and one draw needn't show every extreme that they name: `log_gate_total`: each column never rises from one position to the next.
All inputs are finite; a program needn't handle non-finite values.
Results may differ from a plain program's by a relative error of at most 0.014.
The roundings to bfloat16 on the way count: a program that leaves them out, or rounds other values in their place, can miss the bound.
Values may be sent and summed in bfloat16 or wider, within the bound.
A program may use at most 128 MiB of HBM per device.

v0:
```python
import math

import jax
import jax.numpy as jnp
from jax import lax
from jax.sharding import PartitionSpec as P

NORM_EPS = 1e-06


def head_norm(raw, gain, head_count):
    row_count = raw.shape[0]
    split = raw.reshape(row_count, head_count, -1)
    scaled = split * lax.rsqrt(jnp.mean(split * split, axis=-1, keepdims=True) + NORM_EPS) * gain
    return scaled.reshape(row_count, -1).astype(jnp.bfloat16)


def on_device(
    tokens,
    query_weight,
    key_weight,
    value_weight,
    query_gain,
    key_gain,
    log_gate_total,
    output_weight,
):
    attn_width = query_weight.shape[1]
    head_count = log_gate_total.shape[1]
    head_size = attn_width // head_count
    shard_rows = log_gate_total.shape[0]
    half_rows = shard_rows // 2
    sp_index = lax.axis_index("sp")
    score_scale = head_size ** (-0.5)
    pieces = lax.all_gather(tokens, "tp", axis=0, tiled=True)
    query_part = head_norm(
        jnp.dot(pieces, query_weight, preferred_element_type=jnp.float32), query_gain, head_count
    )
    key_part = head_norm(
        jnp.dot(pieces, key_weight, preferred_element_type=jnp.float32), key_gain, head_count
    )
    value_part = jnp.dot(pieces, value_weight, preferred_element_type=jnp.float32).astype(
        jnp.bfloat16
    )
    joined = jnp.stack([query_part, key_part, value_part], axis=0)
    queries = joined[0]
    key_value = joined[1:]
    gates_all = lax.all_gather(log_gate_total, "sp", axis=0, tiled=True)
    offsets = jnp.arange(shard_rows, dtype=jnp.int32)
    query_pos = sp_index * shard_rows + offsets
    query_heads = queries.reshape(shard_rows, head_count, head_size)
    gate_rows = log_gate_total.T
    halves = []
    for lower in (0, half_rows):
        pos_half = query_pos[lower : lower + half_rows]
        halves.append(
            (
                query_heads[lower : lower + half_rows],
                pos_half,
                gate_rows[:, lower : lower + half_rows],
                jnp.max(pos_half),
            )
        )
    half_state = (
        jnp.full((head_count, half_rows), -1e30, jnp.float32),
        jnp.zeros((head_count, half_rows), jnp.float32),
        jnp.zeros((head_count, half_rows, head_size), jnp.float32),
    )
    carry = (half_state, half_state)
    piece = lax.all_gather(key_value, "sp", axis=1, tiled=True)
    piece_rows = piece.shape[1]
    block_rows = math.gcd(piece_rows, 3072)
    block_count = piece_rows // block_rows
    key_blocks = piece[0].reshape(block_count, block_rows, head_count, head_size)
    value_blocks = piece[1].reshape(block_count, block_rows, head_count, head_size)
    gate_blocks = gates_all.reshape(block_count, block_rows, head_count)

    def one_block(state, inputs):
        key_block, value_block, key_gate, block_index = inputs
        block_start = block_index * block_rows
        key_pos = block_start + jnp.arange(block_rows, dtype=jnp.int32)
        key_gate_rows = key_gate.T
        updated = []
        for half_index in range(2):
            query_half, pos_half, gate_half, last_half = halves[half_index]

            def compute(current):
                running_max, running_sum, running_out = current
                scores = (
                    jnp.einsum(
                        "thd,shd->hts", query_half, key_block, preferred_element_type=jnp.float32
                    )
                    * score_scale
                )
                scores = scores + gate_half[:, :, None] - key_gate_rows[:, None, :]
                scores = jnp.where(
                    key_pos[None, None, :] <= pos_half[None, :, None], scores, -jnp.inf
                )
                new_max = jnp.maximum(running_max, jnp.max(scores, axis=2))
                rescale = jnp.exp(running_max - new_max)
                probs = jnp.exp(scores - new_max[:, :, None])
                running_sum = running_sum * rescale + jnp.sum(probs, axis=2)
                running_out = running_out * rescale[:, :, None] + jnp.einsum(
                    "hts,shd->htd",
                    probs.astype(jnp.bfloat16),
                    value_block,
                    preferred_element_type=jnp.float32,
                )
                return (new_max, running_sum, running_out)

            def keep_state(current):
                return current

            updated.append(
                lax.cond(block_start <= last_half, compute, keep_state, state[half_index])
            )
        return ((updated[0], updated[1]), None)

    carry, unused = lax.scan(
        one_block,
        carry,
        (key_blocks, value_blocks, gate_blocks, jnp.arange(block_count, dtype=jnp.int32)),
    )
    early_state, late_state = carry
    running_sum = jnp.concatenate([early_state[1], late_state[1]], axis=1)
    running_out = jnp.concatenate([early_state[2], late_state[2]], axis=1)
    attended = (
        (running_out / running_sum[:, :, None])
        .transpose(1, 0, 2)
        .reshape(shard_rows, attn_width)
        .astype(jnp.bfloat16)
    )
    mixed = lax.psum_scatter(
        jnp.dot(attended, output_weight, preferred_element_type=jnp.float32).astype(jnp.bfloat16),
        "tp",
        scatter_dimension=0,
        tiled=True,
    )
    return mixed


def solution(mesh):
    placed = (
        P(("sp", "tp"), None),
        P(None, "tp"),
        P(None, "tp"),
        P(None, "tp"),
        P(),
        P(),
        P("sp", "tp"),
        P("tp", None),
    )
    return jax.shard_map(
        on_device, mesh=mesh, in_specs=placed, out_specs=P(("sp", "tp"), None), check_vma=False
    )
```

profile of v0, /device:TPU:29, one launch (start us, length us, event | category | flops | bytes accessed | tf_op | source)
XLA Modules:
  0.0 425.0 jit_solution(7298764967293465248)
XLA Ops:
  8.0 12.3 %all-gather.3.cloned.1.call-done = bf16[384,2048]{1,0:T(8,128)(2,1)} async-done(((bf16[192,2048]{1,0:T(8,128)(2,1)}), bf16[384,2048]{1,0:T(8,128)(2,1)}) %all-gather.3.cloned.1.call-update) | async-done | bytes 1572880 | tf_op jit(solution)/shard_map/all_gather | solution.py:35
  20.4 4.2 fusion.28
  24.6 1.4 copy.13
  26.0 0.9 mul.100
  27.0 1.4 copy.14
  28.4 1.3 fusion.24
  29.7 3.0 fusion.22
  32.7 0.9 pad_maximum_fusion
  33.9 30.2 %all_gather.11 = f32[6144,8]{0,1:T(8,128)S(1)} all-gather(f32[384,8]{0,1:T(8,128)S(1)} %copy-done.7), channel_id=1, replica_groups=mesh['sp'=16,'tp'=2] {'sp'}, dimensions={0}, use_global_device_ids=true | all-gather | bytes 208896 | tf_op jit(solution)/shard_map/all_gather | solution.py:48
  64.9 4.2 fusion.29
  69.1 1.4 copy.17
  70.6 1.0 mul.109
  71.6 1.4 copy.18
  73.0 1.3 multiply_convert_fusion
  74.5 0.8 copy.20
  75.4 109.7 %all-gather.5.cloned.1.call-done = bf16[2,6144,512]{2,1,0:T(8,128)(2,1)} async-done(((bf16[2,384,512]{2,1,0:T(8,128)(2,1)}), bf16[2,6144,512]{2,1,0:T(8,128)(2,1)}) %all-gather.5.cloned.1.call-update) | async-done | bytes 12582928 | tf_op jit(solution)/shard_map/all_gather | solution.py:70
  185.1 10.1 %fusion.25 = (bf16[1,6144,512]{2,1,0:T(8,128)(2,1)}, bf16[1,6144,512]{2,1,0:T(8,128)(2,1)}) fusion(bf16[2,6144,512]{2,1,0:T(8,128)(2,1)} %all-gather.5.cloned.1.call-done), kind=kLoop, calls=%fused_computation.47 | loop fusion | bytes 25165824 | tf_op jit(solution)/shard_map/slice | solution.py:75
  195.2 16.2 %reshape.111 = bf16[2,3072,8,64]{3,2,1,0:T(8,128)(2,1)} reshape(bf16[1,6144,512]{2,1,0:T(8,128)(2,1)} %get-tuple-element.276) | data formatting | bytes 12582912 | tf_op jit(solution)/shard_map/reshape;squeeze | solution.py:74
  211.4 14.1 %copy.21 = bf16[2,3072,8,64]{1,3,2,0:T(8,128)(2,1)} copy(bf16[2,3072,8,64]{3,2,1,0:T(8,128)(2,1)} %reshape.111) | data formatting | bytes 12582912 | tf_op jit(solution)/shard_map/while | solution.py:119
  225.6 16.2 %reshape.112 = bf16[2,3072,8,64]{3,2,1,0:T(8,128)(2,1)} reshape(bf16[1,6144,512]{2,1,0:T(8,128)(2,1)} %get-tuple-element.275) | data formatting | bytes 12582912 | tf_op jit(solution)/shard_map/reshape;squeeze | solution.py:75
  241.8 14.0 %copy.22 = bf16[2,3072,8,64]{1,3,2,0:T(8,128)(2,1)} copy(bf16[2,3072,8,64]{3,2,1,0:T(8,128)(2,1)} %reshape.112) | data formatting | bytes 12582912 | tf_op jit(solution)/shard_map/while | solution.py:119
  255.9 0.8 broadcast_in_dim.48.clone
  256.7 148.3 %while.20 = (s32[]{:T(128)}, f32[8,192]{1,0:T(8,128)S(1)}, f32[8,192]{1,0:T(8,128)S(1)}, f32[8,192,64]{1,2,0:T(8,128)S(1)}, f32[8,192]{1,0:T(8,128)S(1)}, /*inde...) while((s32[]{:T(128)}, f32[8,192]{1,0:T(8,128)S(1)}, ...), condition=%wide.region_13.14_spmd, body=%wide.region_4.13_spmd.sunk | while | flops 2577933312 | bytes 325462240 | solution.py:119
  258.7 6.2 %dynamic-slice_bitcast_fusion.5 = (bf16[3072,8,64]{0,2,1:T(8,128)(2,1)}, bf16[3072,8,64]{0,2,1:T(8,128)(2,1)}) fusion(bf16[2,3072,8,64]{1,3,2,0:T(8,128)(2,1)} %get-tuple-element.483, s32[]{:T(128)S(6)} %copy.46, bf16[2,3072,8,64]{1,3,2,0:T(8,128)(2,1)} %get-tuple-element.481), kind=kLoop, calls=%fused_computation.26.clone.1 | loop fusion | bytes 12582916 | tf_op jit(solution)/shard_map/while/body/jit(dynamic_index_in_dim)/squeeze | solution.py:119
  264.9 32.1 %conditional.4 = ((f32[8,192]{1,0:T(8,128)S(1)}, f32[8,192]{1,0:T(8,128)S(1)}, f32[8,192,64]{1,2,0:T(8,128)S(1)})) conditional(s32[]{:T(128)} %convert_element_type.59, (f32[8,192]{1,0:T(8,128)S(1)}, f32[8,192]{1,0:T(8,128)S(1)}, f32[8,192,64]{1,2,0:T(8,128)S(1)}) %tuple.53, (s32[3072]{0:T(1024)S(1)}, s32[192]{0:T(256)S(1)}, ...), branch_computations={%region_5.5_spmd, %region_6.8_spmd} | conditional | flops 1288965120 | bytes 154762080 | solution.py:115
  265.3 7.2 %fusion.2 = (f32[8,192]{1,0:T(8,128)S(1)}, f32[8,192,3072]{2,1,0:T(8,128)S(1)}) fusion(f32[8,3072]{1,0:T(8,128)S(1)} %get-tuple-element.139, f32[8,192]{1,0:T(8,128)S(1)} %get-tuple-element.138, pred[192,3072]{1,0:T(8,128)(4,1)S(1)} %broadcast_compare_fusion, bf16[192,8,64]{0,2,1:T(8,128)(2,1)S(1)} %get-tuple-element.136, ...), kind=kOutput, calls=%fused_computation.4 | convolution fusion | flops 627571200 | bytes 22917120 | tf_op jit(solution)/shard_map/while/body/eval_jaxpr/cond/branch_1_fun/thd,shd->hts/dot_general | solution.py:90
  272.6 7.3 %copy-done.1 = f32[8,192,3072]{2,1,0:T(8,128)} copy-done((f32[8,192,3072]{2,1,0:T(8,128)}, f32[8,192,3072]{2,1,0:T(8,128)S(1)}, u32[]{:S(2)}) %copy-start.1) | copy-done | bytes 18874392 | tf_op jit(solution)/shard_map/while/body/eval_jaxpr/cond
  279.9 7.2 %fusion.1 = f32[8,192]{1,0:T(8,128)S(1)} fusion(f32[8,192,3072]{2,1,0:T(8,128)S(1)} %get-tuple-element.270, f32[8,192]{1,0:T(8,128)S(1)} %max.4, f32[8,3072]{1,0:T(8,128)S(1)} %get-tuple-element.139, f32[8,192]{1,0:T(8,128)S(1)} %get-tuple-element.138, pred[192,3072]{1,0:T(8,128)(4,1)S(1)} %broadcast_compare_fusion), kind=kLoop, calls=%fused_computation.3 | loop fusion | flops 28310016 | bytes 19580928 | tf_op jit(solution)/shard_map/while/body/eval_jaxpr/cond/branch_1_fun/reduce_sum | solution.py:102
  287.2 9.8 %fusion.6 = f32[8,192,64]{1,2,0:T(8,128)S(1)} fusion(bf16[3072,8,64]{0,2,1:T(8,128)(2,1)S(1)} %copy-done.3, f32[8,192,3072]{2,1,0:T(8,128)} %copy-done.1, f32[8,192]{1,0:T(8,128)S(1)} %max.4, f32[8,3072]{1,0:T(8,128)S(1)} %get-tuple-element.139, f32[8,192]{1,0:T(8,128)S(1)} %get-tuple-element.138, pred[192,3072]{1,0:T(8,128)(4,1)S(1)} %broadcast_compare_fusion, ...), kind=kOutput, calls=%fused_computation.7 | convolution fusion | flops 632487936 | bytes 23513088 | tf_op jit(solution)/shard_map/while/body/eval_jaxpr/cond/branch_1_fun/hts,shd->htd/dot_general | solution.py:103
  297.7 33.2 %conditional.5 = ((f32[8,192]{1,0:T(8,128)S(1)}, f32[8,192]{1,0:T(8,128)S(1)}, f32[8,192,64]{1,2,0:T(8,128)})) conditional(s32[]{:T(128)} %convert_element_type.60, (f32[8,192]{1,0:T(8,128)S(1)}, f32[8,192]{1,0:T(8,128)S(1)}, f32[8,192,64]{1,2,0:T(8,128)}) %tuple.55, (s32[3072]{0:T(1024)S(1)}, s32[192]{0:T(256)S(1)}, bf16[192,8,64]{0,2,1:T(8,128)(2,1)}, ...), branch_computations={%region_9.9_spmd, %region_10.12_spmd} | conditional | flops 1288965120 | bytes 157907872 | solution.py:115
  298.1 7.3 %fusion.13 = (f32[8,192]{1,0:T(8,128)S(1)}, f32[8,192,3072]{2,1,0:T(8,128)S(1)}) fusion(f32[8,3072]{1,0:T(8,128)S(1)} %get-tuple-element.149, f32[8,192]{1,0:T(8,128)S(1)} %get-tuple-element.148, pred[192,3072]{1,0:T(8,128)(4,1)S(1)} %broadcast_compare_fusion.1, bf16[192,8,64]{0,2,1:T(8,128)(2,1)} %get-tuple-element.146, ...), kind=kOutput, calls=%fused_computation.17 | convolution fusion | flops 627571200 | bytes 22917120 | tf_op jit(solution)/shard_map/while/body/eval_jaxpr/cond/branch_1_fun/thd,shd->hts/dot_general | solution.py:90
  305.4 7.5 %copy-done.2 = f32[8,192,3072]{2,1,0:T(8,128)} copy-done((f32[8,192,3072]{2,1,0:T(8,128)}, f32[8,192,3072]{2,1,0:T(8,128)S(1)}, u32[]{:S(2)}) %copy-start.2) | copy-done | bytes 18874392 | tf_op jit(solution)/shard_map/while/body/eval_jaxpr/cond
  313.0 7.2 %fusion.12 = f32[8,192]{1,0:T(8,128)S(1)} fusion(f32[8,192,3072]{2,1,0:T(8,128)S(1)} %get-tuple-element.272, f32[8,192]{1,0:T(8,128)S(1)} %max.5, f32[8,3072]{1,0:T(8,128)S(1)} %get-tuple-element.149, f32[8,192]{1,0:T(8,128)S(1)} %get-tuple-element.148, pred[192,3072]{1,0:T(8,128)(4,1)S(1)} %broadcast_compare_fusion.1), kind=kLoop, calls=%fused_computation.16 | loop fusion | flops 28310016 | bytes 19580928 | tf_op jit(solution)/shard_map/while/body/eval_jaxpr/cond/branch_1_fun/reduce_sum | solution.py:102
  320.2 9.8 %fusion.17 = f32[8,192,64]{1,2,0:T(8,128)S(1)} fusion(bf16[3072,8,64]{0,2,1:T(8,128)(2,1)S(1)} %copy-done.4, f32[8,192,3072]{2,1,0:T(8,128)} %copy-done.2, f32[8,192]{1,0:T(8,128)S(1)} %max.5, f32[8,3072]{1,0:T(8,128)S(1)} %get-tuple-element.149, f32[8,192]{1,0:T(8,128)S(1)} %get-tuple-element.148, pred[192,3072]{1,0:T(8,128)(4,1)S(1)} %broadcast_compare_fusion.1, ...), kind=kOutput, calls=%fused_computation.20 | convolution fusion | flops 632487936 | bytes 23513088 | tf_op jit(solution)/shard_map/while/body/eval_jaxpr/cond/branch_1_fun/hts,shd->htd/dot_general | solution.py:103
  332.9 6.2 %dynamic-slice_bitcast_fusion.5 = (bf16[3072,8,64]{0,2,1:T(8,128)(2,1)}, bf16[3072,8,64]{0,2,1:T(8,128)(2,1)}) fusion(bf16[2,3072,8,64]{1,3,2,0:T(8,128)(2,1)} %get-tuple-element.483, s32[]{:T(128)S(6)} %copy.46, bf16[2,3072,8,64]{1,3,2,0:T(8,128)(2,1)} %get-tuple-element.481), kind=kLoop, calls=%fused_computation.26.clone.1 | loop fusion | bytes 12582916 | tf_op jit(solution)/shard_map/while/body/jit(dynamic_index_in_dim)/squeeze | solution.py:119
  339.1 32.1 %conditional.4 = ((f32[8,192]{1,0:T(8,128)S(1)}, f32[8,192]{1,0:T(8,128)S(1)}, f32[8,192,64]{1,2,0:T(8,128)S(1)})) conditional(s32[]{:T(128)} %convert_element_type.59, (f32[8,192]{1,0:T(8,128)S(1)}, f32[8,192]{1,0:T(8,128)S(1)}, f32[8,192,64]{1,2,0:T(8,128)S(1)}) %tuple.53, (s32[3072]{0:T(1024)S(1)}, s32[192]{0:T(256)S(1)}, ...), branch_computations={%region_5.5_spmd, %region_6.8_spmd} | conditional | flops 1288965120 | bytes 154762080 | solution.py:115
  339.5 7.2 %fusion.2 = (f32[8,192]{1,0:T(8,128)S(1)}, f32[8,192,3072]{2,1,0:T(8,128)S(1)}) fusion(f32[8,3072]{1,0:T(8,128)S(1)} %get-tuple-element.139, f32[8,192]{1,0:T(8,128)S(1)} %get-tuple-element.138, pred[192,3072]{1,0:T(8,128)(4,1)S(1)} %broadcast_compare_fusion, bf16[192,8,64]{0,2,1:T(8,128)(2,1)S(1)} %get-tuple-element.136, ...), kind=kOutput, calls=%fused_computation.4 | convolution fusion | flops 627571200 | bytes 22917120 | tf_op jit(solution)/shard_map/while/body/eval_jaxpr/cond/branch_1_fun/thd,shd->hts/dot_general | solution.py:90
  346.7 7.3 %copy-done.1 = f32[8,192,3072]{2,1,0:T(8,128)} copy-done((f32[8,192,3072]{2,1,0:T(8,128)}, f32[8,192,3072]{2,1,0:T(8,128)S(1)}, u32[]{:S(2)}) %copy-start.1) | copy-done | bytes 18874392 | tf_op jit(solution)/shard_map/while/body/eval_jaxpr/cond
  354.0 7.2 %fusion.1 = f32[8,192]{1,0:T(8,128)S(1)} fusion(f32[8,192,3072]{2,1,0:T(8,128)S(1)} %get-tuple-element.270, f32[8,192]{1,0:T(8,128)S(1)} %max.4, f32[8,3072]{1,0:T(8,128)S(1)} %get-tuple-element.139, f32[8,192]{1,0:T(8,128)S(1)} %get-tuple-element.138, pred[192,3072]{1,0:T(8,128)(4,1)S(1)} %broadcast_compare_fusion), kind=kLoop, calls=%fused_computation.3 | loop fusion | flops 28310016 | bytes 19580928 | tf_op jit(solution)/shard_map/while/body/eval_jaxpr/cond/branch_1_fun/reduce_sum | solution.py:102
  361.3 9.8 %fusion.6 = f32[8,192,64]{1,2,0:T(8,128)S(1)} fusion(bf16[3072,8,64]{0,2,1:T(8,128)(2,1)S(1)} %copy-done.3, f32[8,192,3072]{2,1,0:T(8,128)} %copy-done.1, f32[8,192]{1,0:T(8,128)S(1)} %max.4, f32[8,3072]{1,0:T(8,128)S(1)} %get-tuple-element.139, f32[8,192]{1,0:T(8,128)S(1)} %get-tuple-element.138, pred[192,3072]{1,0:T(8,128)(4,1)S(1)} %broadcast_compare_fusion, ...), kind=kOutput, calls=%fused_computation.7 | convolution fusion | flops 632487936 | bytes 23513088 | tf_op jit(solution)/shard_map/while/body/eval_jaxpr/cond/branch_1_fun/hts,shd->htd/dot_general | solution.py:103
  371.8 33.2 %conditional.5 = ((f32[8,192]{1,0:T(8,128)S(1)}, f32[8,192]{1,0:T(8,128)S(1)}, f32[8,192,64]{1,2,0:T(8,128)})) conditional(s32[]{:T(128)} %convert_element_type.60, (f32[8,192]{1,0:T(8,128)S(1)}, f32[8,192]{1,0:T(8,128)S(1)}, f32[8,192,64]{1,2,0:T(8,128)}) %tuple.55, (s32[3072]{0:T(1024)S(1)}, s32[192]{0:T(256)S(1)}, bf16[192,8,64]{0,2,1:T(8,128)(2,1)}, ...), branch_computations={%region_9.9_spmd, %region_10.12_spmd} | conditional | flops 1288965120 | bytes 157907872 | solution.py:115
  372.2 7.3 %fusion.13 = (f32[8,192]{1,0:T(8,128)S(1)}, f32[8,192,3072]{2,1,0:T(8,128)S(1)}) fusion(f32[8,3072]{1,0:T(8,128)S(1)} %get-tuple-element.149, f32[8,192]{1,0:T(8,128)S(1)} %get-tuple-element.148, pred[192,3072]{1,0:T(8,128)(4,1)S(1)} %broadcast_compare_fusion.1, bf16[192,8,64]{0,2,1:T(8,128)(2,1)} %get-tuple-element.146, ...), kind=kOutput, calls=%fused_computation.17 | convolution fusion | flops 627571200 | bytes 22917120 | tf_op jit(solution)/shard_map/while/body/eval_jaxpr/cond/branch_1_fun/thd,shd->hts/dot_general | solution.py:90
  379.6 7.5 %copy-done.2 = f32[8,192,3072]{2,1,0:T(8,128)} copy-done((f32[8,192,3072]{2,1,0:T(8,128)}, f32[8,192,3072]{2,1,0:T(8,128)S(1)}, u32[]{:S(2)}) %copy-start.2) | copy-done | bytes 18874392 | tf_op jit(solution)/shard_map/while/body/eval_jaxpr/cond
  387.1 7.2 %fusion.12 = f32[8,192]{1,0:T(8,128)S(1)} fusion(f32[8,192,3072]{2,1,0:T(8,128)S(1)} %get-tuple-element.272, f32[8,192]{1,0:T(8,128)S(1)} %max.5, f32[8,3072]{1,0:T(8,128)S(1)} %get-tuple-element.149, f32[8,192]{1,0:T(8,128)S(1)} %get-tuple-element.148, pred[192,3072]{1,0:T(8,128)(4,1)S(1)} %broadcast_compare_fusion.1), kind=kLoop, calls=%fused_computation.16 | loop fusion | flops 28310016 | bytes 19580928 | tf_op jit(solution)/shard_map/while/body/eval_jaxpr/cond/branch_1_fun/reduce_sum | solution.py:102
  394.4 9.8 %fusion.17 = f32[8,192,64]{1,2,0:T(8,128)S(1)} fusion(bf16[3072,8,64]{0,2,1:T(8,128)(2,1)S(1)} %copy-done.4, f32[8,192,3072]{2,1,0:T(8,128)} %copy-done.2, f32[8,192]{1,0:T(8,128)S(1)} %max.5, f32[8,3072]{1,0:T(8,128)S(1)} %get-tuple-element.149, f32[8,192]{1,0:T(8,128)S(1)} %get-tuple-element.148, pred[192,3072]{1,0:T(8,128)(4,1)S(1)} %broadcast_compare_fusion.1, ...), kind=kOutput, calls=%fused_computation.20 | convolution fusion | flops 632487936 | bytes 23513088 | tf_op jit(solution)/shard_map/while/body/eval_jaxpr/cond/branch_1_fun/hts,shd->htd/dot_general | solution.py:103
  405.1 1.3 fusion.23
  406.4 2.2 convolution_convert_fusion
  408.5 9.9 %reduce-scatter.2.cloned.1.call-done = bf16[192,2048]{1,0:T(8,128)(2,1)} async-done(((bf16[384,2048]{1,0:T(8,128)(2,1)}), bf16[192,2048]{1,0:T(8,128)(2,1)}) %reduce-scatter.2.cloned.1.call-update) | async-done | bytes 786448 | tf_op jit(solution)/shard_map/reduce_scatter | solution.py:133
  (74 shorter events, 7.4 us)
Async XLA Ops:
  6.5 399.8 %copy-start = (bf16[512,2048]{1,0:T(8,128)(2,1)S(1)}, bf16[512,2048]{1,0:T(8,128)(2,1)}, u32[]{:S(2)}) copy-start(bf16[512,2048]{1,0:T(8,128)(2,1)} %param.21) | copy-start | bytes 6291460
  6.5 27.2 %copy-start.8 = (f32[64]{0:T(128)S(1)}, f32[64]{0:T(128)}, u32[]{:S(2)}) copy-start(f32[64]{0:T(128)} %param.18) | copy-start | bytes 772
  6.5 27.3 %copy-start.7 = (f32[384,8]{0,1:T(8,128)S(1)}, f32[384,8]{0,1:T(8,128)}, u32[]{:S(2)}) copy-start(f32[384,8]{0,1:T(8,128)} %param.20) | copy-start | bytes 36868
  6.5 13.8 %all-gather.3.cloned.1.call-start = ((), (), s32[]{:S(2)}) async-start(), calls=%async_computation.1 | async-start | bytes 2359296 | tf_op jit(solution)/shard_map/all_gather | solution.py:35
  7.3 177.8 %all-gather.5.cloned.1.call-start = ((), (), s32[]{:S(2)}) async-start(), calls=%async_computation.2 | async-start | bytes 13369344 | tf_op jit(solution)/shard_map/all_gather | solution.py:70
  33.7 384.8 %reduce-scatter.2.cloned.1.call-start = ((), (), s32[]{:S(2)}) async-start(), calls=%async_computation.3 | async-start | bytes 2359296 | tf_op jit(solution)/shard_map/reduce_scatter | solution.py:133
  272.5 7.4 %copy-start.1 = (f32[8,192,3072]{2,1,0:T(8,128)}, f32[8,192,3072]{2,1,0:T(8,128)S(1)}, u32[]{:S(2)}) copy-start(f32[8,192,3072]{2,1,0:T(8,128)S(1)} %get-tuple-element.270) | copy-start | bytes 56623108 | tf_op jit(solution)/shard_map/while/body/eval_jaxpr/cond
  272.5 14.6 %copy-start.3 = (bf16[3072,8,64]{0,2,1:T(8,128)(2,1)S(1)}, bf16[3072,8,64]{0,2,1:T(8,128)(2,1)}, u32[]{:S(2)}) copy-start(bf16[3072,8,64]{0,2,1:T(8,128)(2,1)} %get-tuple-element.142) | copy-start | bytes 9437188 | tf_op jit(solution)/shard_map/while/body/eval_jaxpr/cond
  305.4 7.6 %copy-start.2 = (f32[8,192,3072]{2,1,0:T(8,128)}, f32[8,192,3072]{2,1,0:T(8,128)S(1)}, u32[]{:S(2)}) copy-start(f32[8,192,3072]{2,1,0:T(8,128)S(1)} %get-tuple-element.272) | copy-start | bytes 56623108 | tf_op jit(solution)/shard_map/while/body/eval_jaxpr/cond
  305.4 14.8 %copy-start.4 = (bf16[3072,8,64]{0,2,1:T(8,128)(2,1)S(1)}, bf16[3072,8,64]{0,2,1:T(8,128)(2,1)}, u32[]{:S(2)}) copy-start(bf16[3072,8,64]{0,2,1:T(8,128)(2,1)} %get-tuple-element.152) | copy-start | bytes 9437188 | tf_op jit(solution)/shard_map/while/body/eval_jaxpr/cond
  305.4 14.8 %copy-start.5 = (f32[8,192,64]{1,2,0:T(8,128)S(1)}, f32[8,192,64]{1,2,0:T(8,128)}, u32[]{:S(2)}) copy-start(f32[8,192,64]{1,2,0:T(8,128)} %get-tuple-element.151) | copy-start | bytes 1179652 | tf_op jit(solution)/shard_map/while/body/eval_jaxpr/cond
  330.1 0.8 copy-start.6
  346.7 7.4 %copy-start.1 = (f32[8,192,3072]{2,1,0:T(8,128)}, f32[8,192,3072]{2,1,0:T(8,128)S(1)}, u32[]{:S(2)}) copy-start(f32[8,192,3072]{2,1,0:T(8,128)S(1)} %get-tuple-element.270) | copy-start | bytes 56623108 | tf_op jit(solution)/shard_map/while/body/eval_jaxpr/cond
  346.7 14.6 %copy-start.3 = (bf16[3072,8,64]{0,2,1:T(8,128)(2,1)S(1)}, bf16[3072,8,64]{0,2,1:T(8,128)(2,1)}, u32[]{:S(2)}) copy-start(bf16[3072,8,64]{0,2,1:T(8,128)(2,1)} %get-tuple-element.142) | copy-start | bytes 9437188 | tf_op jit(solution)/shard_map/while/body/eval_jaxpr/cond
  379.5 7.6 %copy-start.2 = (f32[8,192,3072]{2,1,0:T(8,128)}, f32[8,192,3072]{2,1,0:T(8,128)S(1)}, u32[]{:S(2)}) copy-start(f32[8,192,3072]{2,1,0:T(8,128)S(1)} %get-tuple-element.272) | copy-start | bytes 56623108 | tf_op jit(solution)/shard_map/while/body/eval_jaxpr/cond
  379.5 14.8 %copy-start.4 = (bf16[3072,8,64]{0,2,1:T(8,128)(2,1)S(1)}, bf16[3072,8,64]{0,2,1:T(8,128)(2,1)}, u32[]{:S(2)}) copy-start(bf16[3072,8,64]{0,2,1:T(8,128)(2,1)} %get-tuple-element.152) | copy-start | bytes 9437188 | tf_op jit(solution)/shard_map/while/body/eval_jaxpr/cond
  379.6 14.8 %copy-start.5 = (f32[8,192,64]{1,2,0:T(8,128)S(1)}, f32[8,192,64]{1,2,0:T(8,128)}, u32[]{:S(2)}) copy-start(f32[8,192,64]{1,2,0:T(8,128)} %get-tuple-element.151) | copy-start | bytes 1179652 | tf_op jit(solution)/shard_map/while/body/eval_jaxpr/cond
  404.2 0.8 copy-start.6
Sparse Core Ops, SparseCore 0:
  8.9 11.4 all-gather.2
  33.8 151.2 all-gather.4
  408.7 9.7 reduce-scatter.1
where the time goes:
time: 428 us; the launch traced here: 425 us
  waiting for transfers between devices  133 us (31%)
  local copies, waits for them, and re-layouts  126 us (29%)
  matrix products  82 us (19%)
  other arithmetic  36.2 us (8%)
  blocking collectives  30.2 us (7%)
  between operations  13.3 us (3%)
  loops' own time  4.48 us (1%)
    all_gather x1, waiting for transfers between devices, on_device(): piece = lax.all_gather(key_value, 'sp', axis=1, tiled=True)  110 us
    dot_general x4, matrix products, compute(): jnp.einsum('hts,shd->htd', probs.astype(jnp.bfloat16), value_block, prefe...  39.4 us
    cond x28, local copies, waits for them, and re-layouts  31.4 us
    all_gather x1, blocking collectives, on_device(): gates_all = lax.all_gather(log_gate_total, 'sp', axis=0, tiled=True)  30.2 us
    dot_general x4, matrix products, compute(): jnp.einsum('thd,shd->hts', query_half, key_block, preferred_element_type=...  29 us
    reduce_sum x4, other arithmetic, compute(): running_sum = running_sum * rescale + jnp.sum(probs, axis=2)  28.8 us
    while x2, local copies, waits for them, and re-layouts, on_device(): lax.scan(one_block, carry, (key_blocks, value_blocks, gate_blocks, jnp.ar...  28.2 us
    another operation x1, local copies, waits for them, and re-layouts, on_device(): piece[0].reshape(block_count, block_rows, head_count, head_size)  16.2 us
  transfers between devices with their start and end apart: 3, of which 3 were waited for; matrix products, arithmetic and copies ran while one was open for 3% of the time, Pallas kernels for 0%

commit v1 on v0

v1 whole, which is shorter than its diff:
```python
import functools
import math

import jax
import jax.numpy as jnp
from jax import lax
from jax.experimental import pallas as pl
from jax.experimental.pallas import tpu as pltpu
from jax.sharding import PartitionSpec as P

NORM_EPS = 1e-06
LANES = 128
GATE_ROWS = 16
F32 = jnp.float32
BF16 = jnp.bfloat16
MESH = pl.DeviceIdType.MESH


def split3(value):
    first = value.astype(BF16).astype(F32)
    rest = value - first
    second = rest.astype(BF16).astype(F32)
    third = (rest - second).astype(BF16).astype(F32)
    return first, second, third


def kernel(
    n_sp, n_tp, heads, size, shard_rows, tile, block,
    tok_ref, wq_ref, wk_ref, wv_ref, qg_ref, kg_ref, gate_ref, wo_ref,
    out_ref,
    tok_all, wq, wk, wv, wo, stage, slab, kbuf, vbuf, att_stage, att_all, att_rows, part, part_in,
    w_sem, tok_send, tok_recv, slab_send, slab_recv, fwd_send, att_send, att_recv, part_send, part_recv,
):
    me = lax.axis_index("sp")
    tp = lax.axis_index("tp")
    core = lax.rem(tp, 2)
    pair = tp - core
    own_rows = tok_ref.shape[0]
    width = heads * size
    copies = n_sp // (2 * heads)
    k_row = size + GATE_ROWS
    v_row = 2 * k_row
    head_of_chip = me // copies
    src_tp = pair + head_of_chip // heads
    src_head = lax.rem(head_of_chip, heads)
    rank = lax.rem(me, copies) * 2 + core
    group = 2 * copies
    tokens_total = n_sp * shard_rows
    rounds = tokens_total // tile // group
    per_tile = tile // LANES
    per_chunk = shard_rows // LANES

    loads = [
        pltpu.make_async_copy(src, dst, w_sem.at[at])
        for at, (src, dst) in enumerate(
            ((wq_ref, wq), (wk_ref, wk), (wv_ref, wv), (wo_ref, wo), (tok_ref, tok_all.at[tp]))
        )
    ]

    def tok_copy(step):
        peer = lax.rem(tp + step, n_tp)
        return pltpu.make_async_remote_copy(
            src_ref=tok_ref, dst_ref=tok_all.at[tp],
            send_sem=tok_send.at[step], recv_sem=tok_recv.at[step],
            device_id=(me, peer), device_id_type=MESH,
        )

    tok_copies = [tok_copy(step) for step in range(1, n_tp)]
    for copy in tok_copies:
        copy.start()
    loads[4].start()
    for load in loads[:4]:
        load.start()

    row = lax.broadcasted_iota(jnp.int32, (GATE_ROWS, shard_rows), 0)
    for h in range(heads):
        a, b, c = split3(gate_ref[h : h + 1, :])
        one = jnp.ones((GATE_ROWS, shard_rows), F32)
        zero = jnp.zeros((GATE_ROWS, shard_rows), F32)
        first = jnp.where(row == 0, a, jnp.where(row == 1, b, jnp.where(row == 2, c, zero)))
        k_side = jnp.where((row >= 3) & (row < 6), one, first)
        later = jnp.where(row == 3, a, jnp.where(row == 4, b, jnp.where(row == 5, c, zero)))
        q_side = jnp.where(row < 3, -one, later)
        stage[h, size : size + GATE_ROWS, :] = q_side.astype(BF16)
        stage[h, k_row + size : k_row + size + GATE_ROWS, :] = k_side.astype(BF16)

    loads[4].wait()
    for copy in tok_copies:
        copy.wait()

    def slab_copy(h, r, source):
        chip = (core * heads + h) * copies + r
        target = pair + lax.rem(source, 2)
        return chip, target, pltpu.make_async_remote_copy(
            src_ref=stage.at[h], dst_ref=slab.at[source],
            send_sem=slab_send.at[h * copies + r], recv_sem=slab_recv.at[source],
            device_id=(chip, target), device_id_type=MESH,
        )

    def slab_local(h):
        return pltpu.make_async_copy(stage.at[h], slab.at[me], slab_recv.at[me])

    for load in loads[:3]:
        load.wait()

    cols = math.gcd(width, 256)
    group_heads = cols // size

    def project(j, carry):
        at = pl.ds(pl.multiple_of(j * cols, cols), cols)
        for base, weight, gain in ((0, wq, qg_ref), (k_row, wk, kg_ref), (v_row, wv, None)):
            raw = jnp.dot(
                tok_all[...].reshape(n_tp * own_rows, tok_all.shape[2]), weight[:, at],
                preferred_element_type=F32,
            )
            flat = raw.T
            for g in range(group_heads):
                part_t = flat[g * size : (g + 1) * size, :]
                if gain is not None:
                    mean = jnp.mean(part_t * part_t, axis=0, keepdims=True)
                    part_t = part_t * lax.rsqrt(mean + NORM_EPS) * gain[...]
                stage[j * group_heads + g, base : base + size, :] = part_t.astype(BF16)

        def send(at_send, carry):
            h = j * group_heads + at_send // copies
            r = lax.rem(at_send, copies)
            chip, target, copy = slab_copy(h, r, me)
            mine = (chip == me) & (target == tp)

            @pl.when(jnp.logical_not(mine))
            def _():
                copy.start()

            @pl.when(mine)
            def _():
                slab_local(h).start()

            return carry

        lax.fori_loop(0, group_heads * copies, send, 0)
        return carry

    lax.fori_loop(0, width // cols, project, 0)

    def fwd_copy(source):
        return pltpu.make_async_remote_copy(
            src_ref=slab.at[source], dst_ref=slab.at[source],
            send_sem=fwd_send.at[source], recv_sem=slab_recv.at[source],
            device_id=(me, pair + 1 - core), device_id_type=MESH,
        )

    def take(k, carry):
        source = 2 * k + core
        fwd_copy(source).wait_recv()
        fwd_copy(source).start()
        return carry

    lax.fori_loop(0, n_sp // 2, take, 0)

    def take_sibling(k, carry):
        fwd_copy(2 * k + 1 - core).wait_recv()
        return carry

    lax.fori_loop(0, n_sp // 2, take_sibling, 0)

    def prepare(i, carry):
        at = pl.ds(pl.multiple_of(i * shard_rows, shard_rows), shard_rows)
        kbuf[at, :] = slab[i, k_row : k_row + LANES, :].T
        vbuf[:, at] = slab[i, v_row : v_row + size, :]
        return carry

    lax.fori_loop(0, n_sp, prepare, 0)

    def att_copy(g, slot):
        owner = g // per_chunk
        where_to = lax.rem(g, per_chunk)
        return owner, pltpu.make_async_remote_copy(
            src_ref=att_stage.at[slot], dst_ref=att_all.at[src_head, where_to],
            send_sem=att_send.at[slot], recv_sem=att_recv.at[src_head * per_chunk + where_to],
            device_id=(owner, src_tp), device_id_type=MESH,
        )

    def att_local(g, slot):
        where_to = lax.rem(g, per_chunk)
        return pltpu.make_async_copy(
            att_stage.at[slot], att_all.at[src_head, where_to],
            att_recv.at[src_head * per_chunk + where_to],
        )

    def tile_of(k):
        return k * group + jnp.where(lax.rem(k, 2) == 0, rank, group - 1 - rank)

    def attend(k, carry):
        j = tile_of(k)
        pieces = []
        for p in range(per_tile):
            g = j * per_tile + p
            lane = pl.ds(pl.multiple_of(lax.rem(g, per_chunk) * LANES, LANES), LANES)
            pieces.append(slab[g // per_chunk, 0:k_row, lane])
        q = jnp.concatenate(pieces, axis=1)
        q = jnp.concatenate([q, jnp.zeros((LANES - k_row, tile), BF16)], axis=0)

        def step(i, state, masked):
            top, total, acc = state
            at = pl.ds(pl.multiple_of(i * block, block), block)
            s = jnp.dot(kbuf[at, :], q, preferred_element_type=F32)
            if masked:
                key = i * block + lax.broadcasted_iota(jnp.int32, (block, tile), 0)
                query = j * tile + lax.broadcasted_iota(jnp.int32, (block, tile), 1)
                s = jnp.where(key <= query, s, -jnp.inf)
            new_top = jnp.maximum(top, jnp.max(s, axis=0, keepdims=True))
            p = jnp.exp(s - new_top)
            scale = jnp.exp(top - new_top)
            total = total * scale + jnp.sum(p, axis=0, keepdims=True)
            acc = acc * scale + jnp.dot(vbuf[:, at], p.astype(BF16), preferred_element_type=F32)
            return new_top, total, acc

        state = (
            jnp.full((1, tile), -1e30, F32),
            jnp.zeros((1, tile), F32),
            jnp.zeros((size, tile), F32),
        )
        full = j * tile // block
        state = lax.fori_loop(0, full, lambda i, st: step(i, st, False), state)
        top, total, acc = step(full, state, True)
        done = (acc / total).astype(BF16)
        for p in range(per_tile):
            slot = k * per_tile + p
            att_stage[slot] = done[:, p * LANES : (p + 1) * LANES]
        for p in range(per_tile):
            slot = k * per_tile + p
            g = j * per_tile + p
            owner, copy = att_copy(g, slot)
            mine = (owner == me) & (src_tp == tp)

            @pl.when(jnp.logical_not(mine))
            def _():
                copy.start()

            @pl.when(mine)
            def _():
                att_local(g, slot).start()

        return carry

    lax.fori_loop(0, rounds, attend, 0)

    loads[3].wait()

    def att_wait(at, carry):
        h = at // per_chunk
        p = lax.rem(at, per_chunk)
        pltpu.make_async_remote_copy(
            src_ref=att_stage.at[0], dst_ref=att_all.at[h, p],
            send_sem=att_send.at[0], recv_sem=att_recv.at[at],
            device_id=(me, pair + 1 - core), device_id_type=MESH,
        ).wait_recv()
        return carry

    lax.fori_loop(0, heads * per_chunk, att_wait, 0)
    for p in range(per_chunk):
        joined = jnp.concatenate([att_all[h, p] for h in range(heads)], axis=0)
        att_rows[p * LANES : (p + 1) * LANES, :] = joined.T

    def part_copy(step):
        peer = lax.rem(tp + step, n_tp)
        return pltpu.make_async_remote_copy(
            src_ref=part.at[peer], dst_ref=part_in.at[step],
            send_sem=part_send.at[step], recv_sem=part_recv.at[step],
            device_id=(me, peer), device_id_type=MESH,
        )

    model = wo.shape[1]
    out_cols = math.gcd(model, 512)

    def project_rows(step, carry):
        peer = lax.rem(tp + step, n_tp)
        rows = att_rows[pl.ds(pl.multiple_of(peer * own_rows, math.gcd(own_rows, LANES)), own_rows), :]

        def columns(c, carry):
            at = pl.ds(pl.multiple_of(c * out_cols, out_cols), out_cols)
            part[peer, :, at] = jnp.dot(rows, wo[:, at], preferred_element_type=F32).astype(BF16)
            return carry

        lax.fori_loop(0, model // out_cols, columns, 0)
        return carry

    for step in range(1, n_tp):
        project_rows(step, 0)
        part_copy(step).start()
    project_rows(0, 0)
    for step in range(1, n_tp):
        part_copy(step).wait_recv()

    def finish(c, carry):
        at = pl.ds(pl.multiple_of(c * out_cols, out_cols), out_cols)
        mixed = part[tp, :, at].astype(F32)
        for step in range(1, n_tp):
            mixed = mixed + part_in[step, :, at].astype(F32)
        out_ref[:, at] = mixed.astype(BF16)
        return carry

    lax.fori_loop(0, model // out_cols, finish, 0)

    for step in range(1, n_tp):
        part_copy(step).wait_send()

    def sent_slab(at_send, carry):
        h = at_send // copies
        r = lax.rem(at_send, copies)
        chip, target, copy = slab_copy(h, r, me)

        @pl.when(jnp.logical_not((chip == me) & (target == tp)))
        def _():
            copy.wait_send()

        return carry

    lax.fori_loop(0, heads * copies, sent_slab, 0)

    def sent_fwd(k, carry):
        fwd_copy(2 * k + core).wait_send()
        return carry

    lax.fori_loop(0, n_sp // 2, sent_fwd, 0)

    def sent_att(k, carry):
        j = tile_of(k)
        for p in range(per_tile):
            owner, copy = att_copy(j * per_tile + p, k * per_tile + p)

            @pl.when(jnp.logical_not((owner == me) & (src_tp == tp)))
            def _():
                copy.wait_send()

        return carry

    lax.fori_loop(0, rounds, sent_att, 0)


def on_device(n_sp, n_tp, tokens, wq, wk, wv, q_gain, k_gain, gates, wo):
    own_rows, model = tokens.shape
    shard_rows, heads = gates.shape
    width = wq.shape[1]
    size = width // heads
    copies = n_sp // (2 * heads)
    total = n_sp * shard_rows
    tile, block = 256, 512
    rounds = total // tile // (2 * copies)
    slab_rows = 3 * size + 2 * GATE_ROWS
    per_tile = tile // LANES
    per_chunk = shard_rows // LANES
    hbm = pl.BlockSpec(memory_space=pl.ANY)
    vmem = pl.BlockSpec(memory_space=pltpu.VMEM)
    dma = pltpu.SemaphoreType.DMA
    return pl.pallas_call(
        functools.partial(kernel, n_sp, n_tp, heads, size, shard_rows, tile, block),
        out_shape=jax.ShapeDtypeStruct((own_rows, model), BF16),
        in_specs=[hbm, hbm, hbm, hbm, vmem, vmem, vmem, hbm],
        out_specs=vmem,
        scratch_shapes=[
            pltpu.VMEM((n_tp, own_rows, model), BF16),
            pltpu.VMEM(wq.shape, BF16),
            pltpu.VMEM(wk.shape, BF16),
            pltpu.VMEM(wv.shape, BF16),
            pltpu.VMEM(wo.shape, BF16),
            pltpu.VMEM((heads, slab_rows, shard_rows), BF16),
            pltpu.VMEM((n_sp, slab_rows, shard_rows), BF16),
            pltpu.VMEM((total, LANES), BF16),
            pltpu.VMEM((size, total), BF16),
            pltpu.VMEM((rounds * per_tile, size, LANES), BF16),
            pltpu.VMEM((heads, per_chunk, size, LANES), BF16),
            pltpu.VMEM((shard_rows, width), BF16),
            pltpu.VMEM((n_tp, own_rows, model), BF16),
            pltpu.VMEM((n_tp, own_rows, model), BF16),
            dma((5,)),
            dma((n_tp,)),
            dma((n_tp,)),
            dma((heads * copies,)),
            dma((n_sp,)),
            dma((n_sp,)),
            dma((rounds * per_tile,)),
            dma((heads * per_chunk,)),
            dma((n_tp,)),
            dma((n_tp,)),
        ],
        compiler_params=pltpu.CompilerParams(
            has_side_effects=True, vmem_limit_bytes=60 * 1024 * 1024
        ),
    )(
        tokens, wq, wk, wv,
        (q_gain * size ** (-0.5)).reshape(size, 1), k_gain.reshape(size, 1),
        gates.T, wo,
    )


def solution(mesh):
    placed = (
        P(("sp", "tp"), None),
        P(None, "tp"),
        P(None, "tp"),
        P(None, "tp"),
        P(),
        P(),
        P("sp", "tp"),
        P("tp", None),
    )
    return jax.shard_map(
        functools.partial(on_device, mesh.shape["sp"], mesh.shape["tp"]),
        mesh=mesh, in_specs=placed, out_specs=P(("sp", "tp"), None), check_vma=False,
    )
```

time: 428 us -> 106 us (0.25)
  waiting for transfers between devices: 133 us -> 0 us
  local copies, waits for them, and re-layouts: 126 us -> 4.14 us
  Pallas kernels: 0 us -> 101 us
  matrix products: 82 us -> 0 us
  other arithmetic: 36.2 us -> 0.66 us
  blocking collectives: 30.2 us -> 0 us
  between operations: 13.3 us -> 0.01 us
  loops' own time: 4.48 us -> 0 us
    all_gather x2 -> x0, waiting for transfers between devices: 122 us -> none  [the longest x1 110 us: on_device(): piece = lax.all_gather(key_value, 'sp', axis=1, tiled=True)]
    pallas_call x0 -> x1, Pallas kernels: none -> 101 us  [on_device(): pl.pallas_call(functools.partial(kernel, n_sp, n_tp, heads, size, shard_r...]
    dot_general x12 -> x0, matrix products: 82 us -> none  [the longest x4 39.4 us: compute(): jnp.einsum('hts,shd->htd', probs.astype(jnp.bfloat16), value_block, prefe...]
    another operation x2 -> x0, local copies, waits for them, and re-layouts: 32.5 us -> none  [the longest x1 16.2 us: on_device(): piece[0].reshape(block_count, block_rows, head_count, head_size)]
    cond x28 -> x0, local copies, waits for them, and re-layouts: 31.4 us -> none
    all_gather x1 -> x0, blocking collectives: 30.2 us -> none  [on_device(): gates_all = lax.all_gather(log_gate_total, 'sp', axis=0, tiled=True)]
    reduce_sum x6 -> x0, other arithmetic: 28.9 us -> none  [the longest x4 28.8 us: compute(): running_sum = running_sum * rescale + jnp.sum(probs, axis=2)]
    while x2 -> x0, local copies, waits for them, and re-layouts: 28.2 us -> none  [on_device(): lax.scan(one_block, carry, (key_blocks, value_blocks, gate_blocks, jnp.ar...]
  transfers between devices with their start and end apart: 3 -> 0, of which waited for: 3 -> 0; matrix products, arithmetic and copies ran while one was open for 3% -> 0% of each run, Pallas kernels for 0% -> 0%
where the time goes in v1:
time: 106 us
  Pallas kernels  101 us (95%)
  local copies, waits for them, and re-layouts  4.14 us (4%)
    pallas_call x1, Pallas kernels, on_device(): pl.pallas_call(functools.partial(kernel, n_sp, n_tp, heads, size, shard_r...  101 us

profile of v1, /device:TPU:29, one launch (start us, length us, event | category | flops | bytes accessed | tf_op | source)
XLA Modules:
  0.0 106.2 jit_solution(12572895725378131287)
XLA Ops:
  0.0 0.7 multiply_bitcast_fusion
  0.7 0.7 copy.9.qg_ref
  1.4 1.3 %copy.10.kg_ref = f32[64,1]{1,0:T(8,128)} copy(f32[64,1]{0,1:T(1,128)} %bitcast.5) | data formatting | bytes 512 | tf_op jit(solution)/shard_map/reshape | solution.py:392
  2.7 101.4 %shard_map.82 = bf16[192,2048]{1,0:T(8,128)(2,1)} custom-call(bf16[192,2048]{1,0:T(8,128)(2,1)} %tok_ref.1, bf16[2048,512]{1,0:T(8,128)(2,1)} %wq_ref.1, bf16[2048,512]{1,0:T(8,128)(2,1)} %wk_ref.1, bf16[2048,512]{1,0:T(8,128)(2,1)} %wv_ref.1, f32[64,1]{1,0:T(8,128)} %copy.9.qg_ref, f32[64,1]{1,0:T(8,128)} %copy.10.kg_ref, f32[8,384]{1,0:T(8,128)} %bitcast.4, ...), custom_call_target="tpu_custom_call" | custom-call | tf_op jit(solution)/shard_map/pallas_call | solution.py:356
  104.1 2.1 %copy.12 = bf16[192,2048]{1,0:T(8,128)(2,1)} copy(bf16[192,2048]{1,0:T(8,128)(2,1)} %shard_map.82) | data formatting | bytes 1572864

commit v2 on v1

--- a/solution.py
+++ b/solution.py
@@ -28,7 +28,7 @@
     n_sp, n_tp, heads, size, shard_rows, tile, block,
     tok_ref, wq_ref, wk_ref, wv_ref, qg_ref, kg_ref, gate_ref, wo_ref,
     out_ref,
-    tok_all, wq, wk, wv, wo, stage, slab, kbuf, vbuf, att_stage, att_all, att_rows, part, part_in,
+    tok_all, wq, wk, wv, wo, stage, slab, kbuf, vbuf, att_stage, att_all, att_rows, part, part_in, even, odd,
     w_sem, tok_send, tok_recv, slab_send, slab_recv, fwd_send, att_send, att_recv, part_send, part_recv,
 ):
     me = lax.axis_index("sp")
@@ -50,6 +50,22 @@
     per_tile = tile // LANES
     per_chunk = shard_rows // LANES
 
+    barrier = pltpu.get_barrier_semaphore()
+
+    def greet(chip, carry):
+        for side in range(2):
+            @pl.when(jnp.logical_not((chip == me) & (side == core)))
+            def _():
+                pl.semaphore_signal(barrier, inc=1, device_id=(chip, pair + side), device_id_type=MESH)
+
+        return carry
+
+    lax.fori_loop(0, n_sp, greet, 0)
+    for step in range(2, n_tp):
+        pl.semaphore_signal(
+            barrier, inc=1, device_id=(me, lax.rem(pair + step, n_tp)), device_id_type=MESH
+        )
+
     loads = [
         pltpu.make_async_copy(src, dst, w_sem.at[at])
         for at, (src, dst) in enumerate(
@@ -66,8 +82,6 @@
         )
 
     tok_copies = [tok_copy(step) for step in range(1, n_tp)]
-    for copy in tok_copies:
-        copy.start()
     loads[4].start()
     for load in loads[:4]:
         load.start()
@@ -84,6 +98,19 @@
         stage[h, size : size + GATE_ROWS, :] = q_side.astype(BF16)
         stage[h, k_row + size : k_row + size + GATE_ROWS, :] = k_side.astype(BF16)
 
+    eye = lax.broadcasted_iota(jnp.int32, (size, size), 0) == lax.broadcasted_iota(
+        jnp.int32, (size, size), 1
+    )
+
+    def column(ref):
+        return jnp.sum(jnp.where(eye, ref[...], 0.0), axis=1, keepdims=True)
+
+    q_gain = column(qg_ref) * size ** (-0.5)
+    k_gain = column(kg_ref)
+
+    pl.semaphore_wait(barrier, 2 * n_sp - 1 + n_tp - 2)
+    for copy in tok_copies:
+        copy.start()
     loads[4].wait()
     for copy in tok_copies:
         copy.wait()
@@ -108,7 +135,7 @@
 
     def project(j, carry):
         at = pl.ds(pl.multiple_of(j * cols, cols), cols)
-        for base, weight, gain in ((0, wq, qg_ref), (k_row, wk, kg_ref), (v_row, wv, None)):
+        for base, weight, gain in ((0, wq, q_gain), (k_row, wk, k_gain), (v_row, wv, None)):
             raw = jnp.dot(
                 tok_all[...].reshape(n_tp * own_rows, tok_all.shape[2]), weight[:, at],
                 preferred_element_type=F32,
@@ -118,7 +145,7 @@
                 part_t = flat[g * size : (g + 1) * size, :]
                 if gain is not None:
                     mean = jnp.mean(part_t * part_t, axis=0, keepdims=True)
-                    part_t = part_t * lax.rsqrt(mean + NORM_EPS) * gain[...]
+                    part_t = part_t * lax.rsqrt(mean + NORM_EPS) * gain
                 stage[j * group_heads + g, base : base + size, :] = part_t.astype(BF16)
 
         def send(at_send, carry):
@@ -200,16 +227,21 @@
         q = jnp.concatenate(pieces, axis=1)
         q = jnp.concatenate([q, jnp.zeros((LANES - k_row, tile), BF16)], axis=0)
 
-        def step(i, state, masked):
-            top, total, acc = state
+        def produce(ref, i, masked=False):
             at = pl.ds(pl.multiple_of(i * block, block), block)
             s = jnp.dot(kbuf[at, :], q, preferred_element_type=F32)
             if masked:
                 key = i * block + lax.broadcasted_iota(jnp.int32, (block, tile), 0)
                 query = j * tile + lax.broadcasted_iota(jnp.int32, (block, tile), 1)
                 s = jnp.where(key <= query, s, -jnp.inf)
-            new_top = jnp.maximum(top, jnp.max(s, axis=0, keepdims=True))
-            p = jnp.exp(s - new_top)
+            ref[...] = s
+            return jnp.max(s, axis=0, keepdims=True)
+
+        def consume(ref, highest, i, state):
+            top, total, acc = state
+            at = pl.ds(pl.multiple_of(i * block, block), block)
+            new_top = jnp.maximum(top, highest)
+            p = jnp.exp(ref[...] - new_top)
             scale = jnp.exp(top - new_top)
             total = total * scale + jnp.sum(p, axis=0, keepdims=True)
             acc = acc * scale + jnp.dot(vbuf[:, at], p.astype(BF16), preferred_element_type=F32)
@@ -221,8 +253,23 @@
             jnp.zeros((size, tile), F32),
         )
         full = j * tile // block
-        state = lax.fori_loop(0, full, lambda i, st: step(i, st, False), state)
-        top, total, acc = step(full, state, True)
+        high = produce(even, full, True)
+        high_next = produce(odd, 0)
+        state = consume(even, high, full, state)
+
+        def two(i, carry):
+            high, state = carry
+            high_next = produce(even, 2 * i + 1)
+            state = consume(odd, high, 2 * i, state)
+            high = produce(odd, 2 * i + 2)
+            state = consume(even, high_next, 2 * i + 1, state)
+            return high, state
+
+        pairs = full // 2
+        high, state = lax.fori_loop(0, pairs, two, (high_next, state))
+        top, total, acc = lax.fori_loop(
+            2 * pairs, full, lambda i, st: consume(odd, high, i, st), state
+        )
         done = (acc / total).astype(BF16)
         for p in range(per_tile):
             slot = k * per_tile + p
@@ -345,7 +392,7 @@
     size = width // heads
     copies = n_sp // (2 * heads)
     total = n_sp * shard_rows
-    tile, block = 256, 512
+    tile, block = 256, 1024
     rounds = total // tile // (2 * copies)
     slab_rows = 3 * size + 2 * GATE_ROWS
     per_tile = tile // LANES
@@ -373,6 +420,8 @@
             pltpu.VMEM((shard_rows, width), BF16),
             pltpu.VMEM((n_tp, own_rows, model), BF16),
             pltpu.VMEM((n_tp, own_rows, model), BF16),
+            pltpu.VMEM((block, tile), F32),
+            pltpu.VMEM((block, tile), F32),
             dma((5,)),
             dma((n_tp,)),
             dma((n_tp,)),
@@ -385,11 +434,11 @@
             dma((n_tp,)),
         ],
         compiler_params=pltpu.CompilerParams(
-            has_side_effects=True, vmem_limit_bytes=60 * 1024 * 1024
+            has_side_effects=True, collective_id=0, vmem_limit_bytes=60 * 1024 * 1024
         ),
     )(
         tokens, wq, wk, wv,
-        (q_gain * size ** (-0.5)).reshape(size, 1), k_gain.reshape(size, 1),
+        q_gain.reshape(1, size), k_gain.reshape(1, size),
         gates.T, wo,
     )
 

time: 106 us -> 79.5 us (0.75)
  Pallas kernels: 101 us -> 77.1 us
  local copies, waits for them, and re-layouts: 4.14 us -> 2.09 us
    pallas_call x1, Pallas kernels: 101 us -> 77.1 us  [on_device(): pl.pallas_call(functools.partial(kernel, n_sp, n_tp, heads, size, shard_r...]
    reshape x2 -> x0, local copies, waits for them, and re-layouts: 2.05 us -> none  [the longest x1 1.34 us: on_device(): k_gain.reshape(size, 1)]
where the time goes in v2:
time: 79.5 us; the launch traced here: 79.2 us
  Pallas kernels  77.1 us (97%)
  local copies, waits for them, and re-layouts  2.09 us (3%)
    pallas_call x1, Pallas kernels, on_device(): pl.pallas_call(functools.partial(kernel, n_sp, n_tp, heads, size, shard_r...  77.1 us
    unnamed x1, local copies, waits for them, and re-layouts  2.09 us

profile of v2, /device:TPU:29, one launch (start us, length us, event | category | flops | bytes accessed | tf_op | source)
XLA Modules:
  0.0 79.2 jit_solution(1809649232564932004)
XLA Ops:
  0.0 77.1 %shard_map.82 = bf16[192,2048]{1,0:T(8,128)(2,1)} custom-call(bf16[192,2048]{1,0:T(8,128)(2,1)} %tok_ref.1, bf16[2048,512]{1,0:T(8,128)(2,1)} %wq_ref.1, bf16[2048,512]{1,0:T(8,128)(2,1)} %wk_ref.1, bf16[2048,512]{1,0:T(8,128)(2,1)} %wv_ref.1, f32[1,64]{1,0:T(1,128)} %bitcast.4, f32[1,64]{1,0:T(1,128)} %bitcast.5, f32[8,384]{1,0:T(8,128)} %bitcast.3, ...), custom_call_target="tpu_custom_call" | custom-call | tf_op jit(solution)/shard_map/pallas_call | solution.py:403
  77.1 2.1 %copy.10 = bf16[192,2048]{1,0:T(8,128)(2,1)} copy(bf16[192,2048]{1,0:T(8,128)(2,1)} %shard_map.82) | data formatting | bytes 1572864

commit v3 on v2

--- a/solution.py
+++ b/solution.py
@@ -28,7 +28,7 @@
     n_sp, n_tp, heads, size, shard_rows, tile, block,
     tok_ref, wq_ref, wk_ref, wv_ref, qg_ref, kg_ref, gate_ref, wo_ref,
     out_ref,
-    tok_all, wq, wk, wv, wo, stage, slab, kbuf, vbuf, att_stage, att_all, att_rows, part, part_in, even, odd,
+    tok_all, wq, wk, wv, wo, stage, slab, kbuf, vbuf, att_stage, att_all, att_rows, part, part_in, even, odd, kept_top, kept_total, kept_acc,
     w_sem, tok_send, tok_recv, slab_send, slab_recv, fwd_send, att_send, att_recv, part_send, part_recv,
 ):
     me = lax.axis_index("sp")
@@ -38,8 +38,9 @@
     own_rows = tok_ref.shape[0]
     width = heads * size
     copies = n_sp // (2 * heads)
-    k_row = size + GATE_ROWS
-    v_row = 2 * k_row
+    k_row = size
+    gate_row = 2 * size
+    v_row = gate_row + GATE_ROWS
     head_of_chip = me // copies
     src_tp = pair + head_of_chip // heads
     src_head = lax.rem(head_of_chip, heads)
@@ -93,10 +94,7 @@
         zero = jnp.zeros((GATE_ROWS, shard_rows), F32)
         first = jnp.where(row == 0, a, jnp.where(row == 1, b, jnp.where(row == 2, c, zero)))
         k_side = jnp.where((row >= 3) & (row < 6), one, first)
-        later = jnp.where(row == 3, a, jnp.where(row == 4, b, jnp.where(row == 5, c, zero)))
-        q_side = jnp.where(row < 3, -one, later)
-        stage[h, size : size + GATE_ROWS, :] = q_side.astype(BF16)
-        stage[h, k_row + size : k_row + size + GATE_ROWS, :] = k_side.astype(BF16)
+        stage[h, gate_row : gate_row + GATE_ROWS, :] = k_side.astype(BF16)
 
     eye = lax.broadcasted_iota(jnp.int32, (size, size), 0) == lax.broadcasted_iota(
         jnp.int32, (size, size), 1
@@ -176,27 +174,32 @@
             device_id=(me, pair + 1 - core), device_id_type=MESH,
         )
 
-    def take(k, carry):
-        source = 2 * k + core
-        fwd_copy(source).wait_recv()
-        fwd_copy(source).start()
-        return carry
-
-    lax.fori_loop(0, n_sp // 2, take, 0)
-
-    def take_sibling(k, carry):
-        fwd_copy(2 * k + 1 - core).wait_recv()
-        return carry
-
-    lax.fori_loop(0, n_sp // 2, take_sibling, 0)
-
-    def prepare(i, carry):
-        at = pl.ds(pl.multiple_of(i * shard_rows, shard_rows), shard_rows)
-        kbuf[at, :] = slab[i, k_row : k_row + LANES, :].T
-        vbuf[:, at] = slab[i, v_row : v_row + size, :]
-        return carry
-
-    lax.fori_loop(0, n_sp, prepare, 0)
+    half = n_sp // 2
+    upper = me >= half
+
+    def take_half(first):
+        def take(k, carry):
+            source = first + 2 * k + core
+            fwd_copy(source).wait_recv()
+            fwd_copy(source).start()
+            return carry
+
+        lax.fori_loop(0, half // 2, take, 0)
+
+        def take_sibling(k, carry):
+            fwd_copy(first + 2 * k + 1 - core).wait_recv()
+            return carry
+
+        lax.fori_loop(0, half // 2, take_sibling, 0)
+
+        def prepare(k, carry):
+            i = first + k
+            at = pl.ds(pl.multiple_of(i * shard_rows, shard_rows), shard_rows)
+            kbuf[at, :] = slab[i, k_row : k_row + LANES, :].T
+            vbuf[:, at] = slab[i, v_row : v_row + size, :]
+            return carry
+
+        lax.fori_loop(0, half, prepare, 0)
 
     def att_copy(g, slot):
         owner = g // per_chunk
@@ -217,15 +220,31 @@
     def tile_of(k):
         return k * group + jnp.where(lax.rem(k, 2) == 0, rank, group - 1 - rank)
 
-    def attend(k, carry):
+    half_tiles = tokens_total // tile // 2
+    half_blocks = tokens_total // block // 2
+
+    def attend(k, second):
         j = tile_of(k)
-        pieces = []
+        near = (j >= half_tiles) == upper
+        pieces, gates = [], []
         for p in range(per_tile):
             g = j * per_tile + p
             lane = pl.ds(pl.multiple_of(lax.rem(g, per_chunk) * LANES, LANES), LANES)
-            pieces.append(slab[g // per_chunk, 0:k_row, lane])
-        q = jnp.concatenate(pieces, axis=1)
-        q = jnp.concatenate([q, jnp.zeros((LANES - k_row, tile), BF16)], axis=0)
+            pieces.append(slab[g // per_chunk, 0:size, lane])
+            gates.append(slab[g // per_chunk, gate_row : gate_row + GATE_ROWS, lane])
+        q_gate = jnp.concatenate(gates, axis=1).astype(F32)
+        line = lax.broadcasted_iota(jnp.int32, (GATE_ROWS, tile), 0)
+        mixed_gate = jnp.where(line < 3, -1.0, 0.0)
+        for n in range(3):
+            mixed_gate = jnp.where(line == 3 + n, q_gate[n : n + 1, :], mixed_gate)
+        q = jnp.concatenate(
+            [
+                jnp.concatenate(pieces, axis=1),
+                mixed_gate.astype(BF16),
+                jnp.zeros((LANES - size - GATE_ROWS, tile), BF16),
+            ],
+            axis=0,
+        )
 
         def produce(ref, i, masked=False):
             at = pl.ds(pl.multiple_of(i * block, block), block)
@@ -247,29 +266,55 @@
             acc = acc * scale + jnp.dot(vbuf[:, at], p.astype(BF16), preferred_element_type=F32)
             return new_top, total, acc
 
-        state = (
+        fresh = (
             jnp.full((1, tile), -1e30, F32),
             jnp.zeros((1, tile), F32),
             jnp.zeros((size, tile), F32),
         )
         full = j * tile // block
-        high = produce(even, full, True)
-        high_next = produce(odd, 0)
-        state = consume(even, high, full, state)
+
+        def save(state):
+            kept_top[k], kept_total[k], kept_acc[k] = state
+
+        if second:
+            low = 0
+            high_end = jnp.where(near, half_blocks, full)
+
+            @pl.when(jnp.logical_not(near))
+            def _():
+                high = produce(even, full, True)
+                save(consume(even, high, full, fresh))
+
+            high_next = produce(odd, low)
+            state = (kept_top[k], kept_total[k], kept_acc[k])
+        else:
+            low = jnp.where(upper, half_blocks, 0)
+            high_end = full
+            high = produce(even, full, True)
+            high_next = produce(odd, low)
+            state = consume(even, high, full, fresh)
 
         def two(i, carry):
             high, state = carry
-            high_next = produce(even, 2 * i + 1)
-            state = consume(odd, high, 2 * i, state)
-            high = produce(odd, 2 * i + 2)
-            state = consume(even, high_next, 2 * i + 1, state)
+            high_next = produce(even, low + 2 * i + 1)
+            state = consume(odd, high, low + 2 * i, state)
+            high = produce(odd, low + 2 * i + 2)
+            state = consume(even, high_next, low + 2 * i + 1, state)
             return high, state
 
-        pairs = full // 2
+        pairs = (high_end - low) // 2
         high, state = lax.fori_loop(0, pairs, two, (high_next, state))
-        top, total, acc = lax.fori_loop(
-            2 * pairs, full, lambda i, st: consume(odd, high, i, st), state
-        )
+        state = lax.fori_loop(
+            low + 2 * pairs, high_end, lambda i, st: consume(odd, high, i, st), state
+        )
+        if second:
+            emit(k, j, state)
+        else:
+            pl.when(upper)(lambda: save(state))
+            pl.when(jnp.logical_not(upper))(lambda: emit(k, j, state))
+
+    def emit(k, j, state):
+        top, total, acc = state
         done = (acc / total).astype(BF16)
         for p in range(per_tile):
             slot = k * per_tile + p
@@ -288,9 +333,18 @@
             def _():
                 att_local(g, slot).start()
 
-        return carry
-
-    lax.fori_loop(0, rounds, attend, 0)
+    def first_pass(k, carry):
+        pl.when((tile_of(k) >= half_tiles) == upper)(lambda: attend(k, False))
+        return carry
+
+    def second_pass(k, carry):
+        pl.when(upper | (tile_of(k) >= half_tiles))(lambda: attend(k, True))
+        return carry
+
+    take_half(jnp.where(upper, half, 0))
+    lax.fori_loop(0, rounds, first_pass, 0)
+    take_half(jnp.where(upper, 0, half))
+    lax.fori_loop(0, rounds, second_pass, 0)
 
     loads[3].wait()
 
@@ -394,7 +448,7 @@
     total = n_sp * shard_rows
     tile, block = 256, 1024
     rounds = total // tile // (2 * copies)
-    slab_rows = 3 * size + 2 * GATE_ROWS
+    slab_rows = 3 * size + GATE_ROWS
     per_tile = tile // LANES
     per_chunk = shard_rows // LANES
     hbm = pl.BlockSpec(memory_space=pl.ANY)
@@ -422,6 +476,9 @@
             pltpu.VMEM((n_tp, own_rows, model), BF16),
             pltpu.VMEM((block, tile), F32),
             pltpu.VMEM((block, tile), F32),
+            pltpu.VMEM((rounds, 1, tile), F32),
+            pltpu.VMEM((rounds, 1, tile), F32),
+            pltpu.VMEM((rounds, size, tile), F32),
             dma((5,)),
             dma((n_tp,)),
             dma((n_tp,)),

time: 79.5 us -> 73.8 us (0.928)
  Pallas kernels: 77.1 us -> 71.5 us
    pallas_call x1, Pallas kernels: 77.1 us -> 71.5 us  [on_device(): pl.pallas_call(functools.partial(kernel, n_sp, n_tp, heads, size, shard_r...]
where the time goes in v3:
time: 73.8 us; the launch traced here: 73.6 us
  Pallas kernels  71.5 us (97%)
  local copies, waits for them, and re-layouts  2.09 us (3%)
    pallas_call x1, Pallas kernels, on_device(): pl.pallas_call(functools.partial(kernel, n_sp, n_tp, heads, size, shard_r...  71.5 us
    unnamed x1, local copies, waits for them, and re-layouts  2.09 us

profile of v3, /device:TPU:29, one launch (start us, length us, event | category | flops | bytes accessed | tf_op | source)
XLA Modules:
  0.0 73.6 jit_solution(6302064684517303783)
XLA Ops:
  0.0 71.5 %shard_map.82 = bf16[192,2048]{1,0:T(8,128)(2,1)} custom-call(bf16[192,2048]{1,0:T(8,128)(2,1)} %tok_ref.1, bf16[2048,512]{1,0:T(8,128)(2,1)} %wq_ref.1, bf16[2048,512]{1,0:T(8,128)(2,1)} %wk_ref.1, bf16[2048,512]{1,0:T(8,128)(2,1)} %wv_ref.1, f32[1,64]{1,0:T(1,128)} %bitcast.4, f32[1,64]{1,0:T(1,128)} %bitcast.5, f32[8,384]{1,0:T(8,128)} %bitcast.3, ...), custom_call_target="tpu_custom_call" | custom-call | tf_op jit(solution)/shard_map/pallas_call | solution.py:457
  71.5 2.1 %copy.10 = bf16[192,2048]{1,0:T(8,128)(2,1)} copy(bf16[192,2048]{1,0:T(8,128)(2,1)} %shard_map.82) | data formatting | bytes 1572864

commit v4 on v3

--- a/solution.py
+++ b/solution.py
@@ -147,7 +147,7 @@
                 stage[j * group_heads + g, base : base + size, :] = part_t.astype(BF16)
 
         def send(at_send, carry):
-            h = j * group_heads + at_send // copies
+            h = j * group_heads + lax.rem(at_send // copies + me, group_heads)
             r = lax.rem(at_send, copies)
             chip, target, copy = slab_copy(h, r, me)
             mine = (chip == me) & (target == tp)

time: 73.8 us -> 69.3 us (0.939); the launches traced: 73.6 us -> 68.2 us
  Pallas kernels: 71.5 us -> 66.1 us
    pallas_call x1, Pallas kernels: 71.5 us -> 66.1 us  [on_device(): pl.pallas_call(functools.partial(kernel, n_sp, n_tp, heads, size, shard_r...]
where the time goes in v4:
time: 69.3 us; the launch traced here: 68.2 us
  Pallas kernels  66.1 us (95%)
  local copies, waits for them, and re-layouts  2.09 us (3%)
    pallas_call x1, Pallas kernels, on_device(): pl.pallas_call(functools.partial(kernel, n_sp, n_tp, heads, size, shard_r...  66.1 us
    unnamed x1, local copies, waits for them, and re-layouts  2.09 us

profile of v4, /device:TPU:29, one launch (start us, length us, event | category | flops | bytes accessed | tf_op | source)
XLA Modules:
  0.0 68.2 jit_solution(14843608113361942332)
XLA Ops:
  0.0 66.1 %shard_map.82 = bf16[192,2048]{1,0:T(8,128)(2,1)} custom-call(bf16[192,2048]{1,0:T(8,128)(2,1)} %tok_ref.1, bf16[2048,512]{1,0:T(8,128)(2,1)} %wq_ref.1, bf16[2048,512]{1,0:T(8,128)(2,1)} %wk_ref.1, bf16[2048,512]{1,0:T(8,128)(2,1)} %wv_ref.1, f32[1,64]{1,0:T(1,128)} %bitcast.4, f32[1,64]{1,0:T(1,128)} %bitcast.5, f32[8,384]{1,0:T(8,128)} %bitcast.3, ...), custom_call_target="tpu_custom_call" | custom-call | tf_op jit(solution)/shard_map/pallas_call | solution.py:457
  66.1 2.1 %copy.10 = bf16[192,2048]{1,0:T(8,128)(2,1)} copy(bf16[192,2048]{1,0:T(8,128)(2,1)} %shard_map.82) | data formatting | bytes 1572864
